TPU v7x, 512 devices: a whole 4x8x8 slice. The times are simulated.
512 devices in a mesh: dp: 4 (over x), kv: 64 (over z, y), tp: 2 (over core).
Axes of the slice: x: 4, y: 8, z: 8, core: 2. Of those that a mesh axis runs over, the one named last changes fastest.
Arguments:
- tokens: bfloat16 [192, 2048], P(('dp', 'tp'), 'kv'), may hold values from -8 to 8
- mix_gain: float32 [2048], replicated, may hold values from 0.1 to 1.9
- w_gate: bfloat16 [2048, 4096], P(None, 'kv'), may hold values from -0.125 to 0.125
- w_value: bfloat16 [2048, 4096], P(None, 'kv'), may hold values from -0.125 to 0.125
- w_maps: bfloat16 [2048, 16384], P(None, 'kv'), may hold values from -0.125 to 0.125
- w_step: bfloat16 [2048, 64], replicated, may hold values from -0.125 to 0.125
- conv_value: float32 [4, 4096], P(None, 'kv'), may hold values from -0.5 to 0.5
- conv_maps: float32 [4, 16384], P(None, 'kv'), may hold values from -0.5 to 0.5
- past_value: bfloat16 [192, 3, 4096], P(('dp', 'tp'), None, 'kv'), may hold values from -6 to 6
- past_maps: bfloat16 [192, 3, 16384], P(('dp', 'tp'), None, 'kv'), may hold values from -6 to 6
- step_bias: float32 [64], P('kv'), may hold values from -3 to 0
- decay_log: float32 [64], P('kv'), may hold values from 0 to 2.77
- skip_gain: float32 [64], P('kv'), may hold values from 0.1 to 1.9
- head_gain: float32 [4096], P('kv'), may hold values from 0.1 to 1.9
- state: float32 [192, 64, 64, 128], P(('dp', 'tp'), 'kv'), may hold values from -2 to 2
- w_out: bfloat16 [4096, 2048], P('kv'), may hold values from -0.25 to 0.25
- mlp_gain: float32 [2048], replicated, may hold values from 0.1 to 1.9
- w_up: bfloat16 [2048, 8192], P(None, 'kv'), may hold values from -0.125 to 0.125
- w_down: bfloat16 [8192, 2048], P('kv'), may hold values from -0.1875 to 0.1875
Outputs:
- layer_out: bfloat16 [192, 2048], P(('dp', 'tp'), 'kv')
- state_next: float32 [192, 64, 64, 128], P(('dp', 'tp'), 'kv')
- value_tail: bfloat16 [192, 3, 4096], P(('dp', 'tp'), None, 'kv')
- maps_tail: bfloat16 [192, 3, 16384], P(('dp', 'tp'), None, 'kv')
All inputs are finite; a program needn't handle non-finite values.
Results may differ from a plain program's by a relative error of at most 0.0081.
Values may be sent and summed in bfloat16 or wider, within the bound.
A program may use at most 64 MiB of HBM per device.

v0:
```python
import jax
import jax.numpy as jnp
from jax import lax
from jax.sharding import PartitionSpec as P

HEAD_DIM = 64
STATE = 128


NORM_EPS = 1e-05


def joined_along(blocks, dim):
    lengths = list(blocks.shape[1:])
    lengths[dim] *= blocks.shape[0]
    return jnp.moveaxis(blocks, 0, dim).reshape(lengths)


def copy_for_each(shard, axis):
    copies = jnp.broadcast_to(shard, (lax.axis_size(axis), *shard.shape))
    return lax.all_to_all(copies, axis, split_axis=0, concat_axis=0, tiled=True)


def gathered_copies(shard, axis, dim):
    return joined_along(copy_for_each(shard, axis), dim)


def split_up(shard, dim, length):
    lengths = shard.shape
    blocks = shard.reshape(*lengths[:dim], length, lengths[dim] // length, *lengths[dim + 1 :])
    return jnp.moveaxis(blocks, dim, 0)


def sum_at_owner(shard, axis, dim):
    blocks = split_up(shard, dim, lax.axis_size(axis))
    arrived = lax.all_to_all(blocks, axis, split_axis=0, concat_axis=0, tiled=True)
    return arrived.sum(axis=0)


def rms_rows(matrix, gain_vec):
    widened = matrix.astype(jnp.float32)
    inv_scale = lax.rsqrt(jnp.mean(widened * widened, axis=-1, keepdims=True) + NORM_EPS)
    return (widened * inv_scale * gain_vec).astype(jnp.bfloat16)


def short_conv(past_rows, newest, kernel):
    window = jnp.concatenate([past_rows, newest[:, None, :]], axis=1)
    summed = jnp.sum(window.astype(jnp.float32) * kernel[None], axis=1)
    return (jax.nn.silu(summed), window[:, 1:, :])


def local(
    tokens,
    mix_gain,
    w_gate,
    w_value,
    w_maps,
    w_step,
    conv_value,
    conv_maps,
    past_value,
    past_maps,
    step_bias,
    decay_log,
    skip_gain,
    head_gain,
    state,
    w_out,
    mlp_gain,
    w_up,
    w_down,
):
    whole_rows = gathered_copies(tokens, "kv", 1)
    batch_rows = whole_rows.shape[0]
    heads_here = state.shape[1]
    head_start = lax.axis_index("kv") * heads_here
    normed = rms_rows(whole_rows, mix_gain)
    gate_pre = jnp.dot(normed, w_gate, preferred_element_type=jnp.float32)
    step_cols = lax.dynamic_slice_in_dim(w_step, head_start, heads_here, 1)
    step_pre = jnp.dot(normed, step_cols, preferred_element_type=jnp.float32)
    value_new = jnp.dot(normed, w_value, preferred_element_type=jnp.float32).astype(jnp.bfloat16)
    maps_new = jnp.dot(normed, w_maps, preferred_element_type=jnp.float32).astype(jnp.bfloat16)
    value_act, value_tail = short_conv(past_value, value_new, conv_value)
    maps_act, maps_tail = short_conv(past_maps, maps_new, conv_maps)
    maps_act = lax.optimization_barrier(maps_act.astype(jnp.bfloat16))
    grouped = maps_act.astype(jnp.float32).reshape(batch_rows, -1, 2, STATE)
    per_group = heads_here // grouped.shape[1]
    in_map = jnp.repeat(grouped[:, :, 0], per_group, axis=1)
    out_map = jnp.repeat(grouped[:, :, 1], per_group, axis=1)
    head_values = value_act.reshape(batch_rows, heads_here, HEAD_DIM)
    step_size = jax.nn.softplus(step_pre + step_bias)
    decay_rate = jnp.exp(-step_size * jnp.exp(decay_log))
    written = (step_size[:, :, None] * head_values)[:, :, :, None] * in_map[:, :, None, :]
    state_next = decay_rate[:, :, None, None] * state + written
    read_out = (
        jnp.sum(state_next * out_map[:, :, None, :], axis=-1)
        + skip_gain[None, :, None] * head_values
    )
    gated_heads = read_out * jax.nn.silu(gate_pre.reshape(batch_rows, heads_here, HEAD_DIM))
    inv_scale = lax.rsqrt(jnp.mean(gated_heads * gated_heads, axis=-1, keepdims=True) + NORM_EPS)
    heads_out = gated_heads * inv_scale * head_gain.reshape(heads_here, HEAD_DIM)
    heads_out = heads_out.reshape(batch_rows, heads_here * HEAD_DIM).astype(jnp.bfloat16)
    partial_value = jnp.dot(heads_out, w_out, preferred_element_type=jnp.float32)
    own_part = sum_at_owner(partial_value, "kv", 1)
    own_hidden = lax.optimization_barrier(
        (tokens.astype(jnp.float32) + own_part).astype(jnp.bfloat16)
    )
    hidden = gathered_copies(own_hidden, "kv", 1)
    normed_mlp = rms_rows(hidden, mlp_gain)
    squared = jnp.square(jax.nn.relu(jnp.dot(normed_mlp, w_up, preferred_element_type=jnp.float32)))
    squared = squared.astype(jnp.bfloat16)
    partial_mlp = jnp.dot(squared, w_down, preferred_element_type=jnp.float32)
    mlp_part = sum_at_owner(partial_mlp, "kv", 1)
    layer_out = (own_hidden.astype(jnp.float32) + mlp_part).astype(jnp.bfloat16)
    return (layer_out, state_next, value_tail, maps_tail)


def solution(mesh):
    in_specs = (
        P(("dp", "tp"), "kv"),
        P(),
        P(None, "kv"),
        P(None, "kv"),
        P(None, "kv"),
        P(),
        P(None, "kv"),
        P(None, "kv"),
        P(("dp", "tp"), None, "kv"),
        P(("dp", "tp"), None, "kv"),
        P("kv"),
        P("kv"),
        P("kv"),
        P("kv"),
        P(("dp", "tp"), "kv", None, None),
        P("kv", None),
        P(),
        P(None, "kv"),
        P("kv", None),
    )
    out_specs = (
        P(("dp", "tp"), "kv"),
        P(("dp", "tp"), "kv", None, None),
        P(("dp", "tp"), None, "kv"),
        P(("dp", "tp"), None, "kv"),
    )
    return jax.shard_map(local, mesh=mesh, in_specs=in_specs, out_specs=out_specs, check_vma=False)
```

profile of v0, /device:TPU:6, one launch (start us, length us, event | category | flops | bytes accessed | tf_op | source)
XLA Modules:
  0.0 102.7 jit_solution(2187422286288096051)
XLA Ops:
  0.6 0.8 broadcast_in_dim.8
  1.5 1.0 reshape.170
  2.4 16.6 %all-to-all-start = ((bf16[64,2,384]{2,1,0:T(2,128)(2,1)}), bf16[64,2,384]{2,1,0:T(2,128)(2,1)S(1)}, u32[]{:S(2)}, u32[]{:S(2)}) async-start(bf16[64,2,384]{2,1,0:T(2,128)(2,1)} %reshape.170), calls=%async_computation | async-start | bytes 196608 | tf_op jit(solution)/shard_map/all_to_all | solution.py:21
  21.4 10.1 %all-to-all-done = bf16[64,2,384]{2,1,0:T(2,128)(2,1)S(1)} async-done(((bf16[64,2,384]{2,1,0:T(2,128)(2,1)}), bf16[64,2,384]{2,1,0:T(2,128)(2,1)S(1)}, u32[]{:S(2)}, u32[]{:S(2)}) %all-to-all-start) | async-done | bytes 98336 | tf_op jit(solution)/shard_map/all_to_all | solution.py:21
  32.3 1.0 %convert_element_type.74 = bf16[24,2048]{1,0:T(8,128)(2,1)} reshape(bf16[24,64,32]{2,1,0:T(8,128)(2,1)S(1)} %copy.38) | data formatting | bytes 196608 | tf_op jit(solution)/shard_map/convert_element_type | solution.py:43
  33.5 0.4 reshape.162
  34.0 0.9 copy-done.6
  35.3 0.5 copy-done.7
  35.9 0.7 copy-done.10
  36.7 0.9 multiply_exponential_fusion
  37.7 1.2 %multiply_reduce_fusion = (f32[24,64]{1,0:T(8,128)S(1)}, f32[24,1,64,128]{3,2,1,0:T(8,128)}) fusion(f32[24,128]{1,0:T(8,128)S(1)} %bitcast.44, f32[24,128]{1,0:T(8,128)S(1)} %bitcast.43, f32[24,64]{1,0:T(8,128)S(1)} %broadcast_multiply_fusion, f32[24,1,64,128]{3,2,1,0:T(8,128)S(1)} %copy-done.1, f32[24]{0:T(128)S(1)} %get-tuple-element.18), kind=kLoop, calls=%fused_computation.20 | loop fusion | flops 981504 | bytes 1609824 | tf_op jit(solution)/shard_map/reduce_sum | solution.py:96
  38.9 0.3 multiply_reduce_fusion.3
  39.2 0.7 copy-done.19
  39.9 0.5 convolution_bitcast_fusion
  40.4 0.3 copy.42
  40.8 1.0 reshape.172
  41.8 4.7 %all-to-all-start.1 = ((f32[64,1,768]{2,1,0:T(1,128)}), f32[64,1,768]{2,1,0:T(1,128)S(1)}, u32[]{:S(2)}, u32[]{:S(2)}) async-start(f32[64,1,768]{2,1,0:T(1,128)} %reshape.172), calls=%async_computation.1 | async-start | bytes 393216 | tf_op jit(solution)/shard_map/all_to_all | solution.py:36
  46.6 13.2 %all-to-all-done.1 = f32[64,1,768]{2,1,0:T(1,128)S(1)} async-done(((f32[64,1,768]{2,1,0:T(1,128)}), f32[64,1,768]{2,1,0:T(1,128)S(1)}, u32[]{:S(2)}, u32[]{:S(2)}) %all-to-all-start.1) | async-done | bytes 196640 | tf_op jit(solution)/shard_map/all_to_all | solution.py:36
  59.8 0.5 broadcast.127
  60.4 1.1 %reduce.7 = f32[64,768]{1,0:T(8,128)S(1)} reduce(f32[64,1,768]{2,1,0:T(1,128)S(1)} %all-to-all-done.1, f32[]{:T(128)} %broadcast.127), dimensions={1}, to_apply=%all_to_all.13.reduce_sub_computation | reduce | bytes 393220 | tf_op jit(solution)/shard_map/all_to_all | solution.py:36
  62.4 16.3 %all_to_all.20 = bf16[64,2,384]{2,1,0:T(2,128)(2,1)S(1)} all-to-all(bf16[64,2,384]{2,1,0:T(2,128)(2,1)S(1)} %reshape.174), channel_id=1, replica_groups=mesh['dp'=4,'kv'=64,'tp'=2] {'kv'}, dimensions={0} | all-to-all | bytes 196608 | tf_op jit(solution)/shard_map/all_to_all | solution.py:21
  79.4 0.4 reshape.165
  79.7 0.5 copy-done.3
  80.4 0.4 fusion.3
  81.1 0.5 copy.46
  81.5 1.0 reshape.176
  82.6 4.7 %all-to-all-start.3 = ((f32[64,1,768]{2,1,0:T(1,128)}), f32[64,1,768]{2,1,0:T(1,128)S(1)}, u32[]{:S(2)}, u32[]{:S(2)}) async-start(f32[64,1,768]{2,1,0:T(1,128)} %reshape.176), calls=%async_computation.3 | async-start | bytes 393216 | tf_op jit(solution)/shard_map/all_to_all | solution.py:36
  87.3 0.6 fusion.17
  88.1 0.6 fusion.16
  88.7 11.7 %all-to-all-done.3 = f32[64,1,768]{2,1,0:T(1,128)S(1)} async-done(((f32[64,1,768]{2,1,0:T(1,128)}), f32[64,1,768]{2,1,0:T(1,128)S(1)}, u32[]{:S(2)}, u32[]{:S(2)}) %all-to-all-start.3) | async-done | bytes 196640 | tf_op jit(solution)/shard_map/all_to_all | solution.py:36
  100.5 1.1 %reduce.8 = f32[64,768]{1,0:T(8,128)S(1)} reduce(f32[64,1,768]{2,1,0:T(1,128)S(1)} %all-to-all-done.3, f32[]{:T(128)} %broadcast.127), dimensions={1}, to_apply=%all_to_all.15.reduce_sub_computation | reduce | bytes 393220 | tf_op jit(solution)/shard_map/all_to_all | solution.py:36
  102.0 0.7 copy.48
  (72 shorter events, 4.8 us)
Async XLA Ops:
  0.6 34.4 %copy-start = (bf16[2048,256]{1,0:T(8,128)(2,1)S(1)}, bf16[2048,256]{1,0:T(8,128)(2,1)}, u32[]{:S(2)}) copy-start(bf16[2048,256]{1,0:T(8,128)(2,1)} %param.23) | copy-start | bytes 3145732
  1.5 19.7 %copy-start.4 = (bf16[64,2048]{1,0:T(8,128)(2,1)S(1)}, bf16[64,2048]{1,0:T(8,128)(2,1)}, u32[]{:S(2)}) copy-start(bf16[64,2048]{1,0:T(8,128)(2,1)} %param.34) | copy-start | bytes 786436
  2.4 29.1 %all-to-all-start = ((bf16[64,2,384]{2,1,0:T(2,128)(2,1)}), bf16[64,2,384]{2,1,0:T(2,128)(2,1)S(1)}, u32[]{:S(2)}, u32[]{:S(2)}) async-start(bf16[64,2,384]{2,1,0:T(2,128)(2,1)} %reshape.170), calls=%async_computation | async-start | bytes 196608 | tf_op jit(solution)/shard_map/all_to_all | solution.py:21
  19.0 2.0 %copy-start.14 = (f32[2048]{0:T(1024)S(1)}, f32[2048]{0:T(1024)}, u32[]{:S(2)}) copy-start(f32[2048]{0:T(1024)} %param.20) | copy-start | bytes 24580
  33.9 1.0 copy-start.6
  35.0 0.9 copy-start.12
  35.0 0.8 copy-start.7
  35.0 0.8 copy-start.17
  35.0 2.7 %copy-start.1 = (f32[24,1,64,128]{3,2,1,0:T(8,128)S(1)}, f32[24,1,64,128]{3,2,1,0:T(8,128)}, u32[]{:S(2)}) copy-start(f32[24,1,64,128]{3,2,1,0:T(8,128)} %param.33) | copy-start | bytes 2359300
  35.8 0.9 copy-start.9
  35.9 0.7 copy-start.10
  35.9 0.7 copy-start.18
  37.7 1.2 %copy-start.5 = (bf16[2048,64]{0,1:T(8,128)(2,1)S(1)}, bf16[2048,64]{0,1:T(8,128)(2,1)}, u32[]{:S(2)}) copy-start(bf16[2048,64]{0,1:T(8,128)(2,1)} %param.21) | copy-start | bytes 786436
  39.2 0.7 copy-start.19
  41.8 4.7 %copy-start.15 = (bf16[24,32]{1,0:T(8,128)(2,1)S(1)}, bf16[24,32]{1,0:T(8,128)(2,1)}, u32[]{:S(2)}) copy-start(bf16[24,32]{1,0:T(8,128)(2,1)} %param.19) | copy-start | bytes 4612
  41.8 18.1 %all-to-all-start.1 = ((f32[64,1,768]{2,1,0:T(1,128)}), f32[64,1,768]{2,1,0:T(1,128)S(1)}, u32[]{:S(2)}, u32[]{:S(2)}) async-start(f32[64,1,768]{2,1,0:T(1,128)} %reshape.172), calls=%async_computation.1 | async-start | bytes 393216 | tf_op jit(solution)/shard_map/all_to_all | solution.py:36
  79.2 1.0 %copy-start.3 = (bf16[2048,128]{1,0:T(8,128)(2,1)S(1)}, bf16[2048,128]{1,0:T(8,128)(2,1)}, u32[]{:S(2)}) copy-start(bf16[2048,128]{1,0:T(8,128)(2,1)} %param.36) | copy-start | bytes 1572868
  79.3 1.1 %copy-start.2 = (bf16[128,2048]{1,0:T(8,128)(2,1)S(1)}, bf16[128,2048]{1,0:T(8,128)(2,1)}, u32[]{:S(2)}) copy-start(bf16[128,2048]{1,0:T(8,128)(2,1)} %param.37) | copy-start | bytes 1572868
  79.3 1.1 %copy-start.16 = (f32[2048]{0:T(1024)S(1)}, f32[2048]{0:T(1024)}, u32[]{:S(2)}) copy-start(f32[2048]{0:T(1024)} %param.35) | copy-start | bytes 24580
  82.6 4.8 %copy-start.11 = (bf16[24,3,64]{2,0,1:T(8,128)(2,1)S(1)}, bf16[24,3,64]{2,0,1:T(8,128)(2,1)}, u32[]{:S(2)}) copy-start(bf16[24,3,64]{2,0,1:T(8,128)(2,1)} %param.27) | copy-start | bytes 27652
  82.6 4.8 %copy-start.13 = (bf16[24,1,64]{2,0,1:T(8,128)(2,1)S(1)}, bf16[24,1,64]{2,0,1:T(8,128)(2,1)}, u32[]{:S(2)}) copy-start(bf16[24,1,64]{2,0,1:T(8,128)(2,1)} %copy-done.12) | copy-start | bytes 9220
  82.6 17.9 %all-to-all-start.3 = ((f32[64,1,768]{2,1,0:T(1,128)}), f32[64,1,768]{2,1,0:T(1,128)S(1)}, u32[]{:S(2)}, u32[]{:S(2)}) async-start(f32[64,1,768]{2,1,0:T(1,128)} %reshape.176), calls=%async_computation.3 | async-start | bytes 393216 | tf_op jit(solution)/shard_map/all_to_all | solution.py:36
  87.3 0.8 copy-start.8
where the time goes:
time: 103 us
  waiting for transfers between devices  35 us (34%)
  starting transfers between devices  26.1 us (25%)
  blocking collectives  16.3 us (16%)
  local copies, waits for them, and re-layouts  13.9 us (13%)
  other arithmetic  5.82 us (6%)
  between operations  3.03 us (3%)
  matrix products  2.58 us (3%)
    all_to_all x2, waiting for transfers between devices, sum_at_owner(): lax.all_to_all(blocks, axis, split_axis=0, concat_axis=0, tiled=True)  24.9 us
    all_to_all x1, starting transfers between devices, copy_for_each(): return lax.all_to_all(copies, axis, split_axis=0, concat_axis=0, tiled=True)  16.6 us
    all_to_all x1, blocking collectives, copy_for_each(): return lax.all_to_all(copies, axis, split_axis=0, concat_axis=0, tiled=True)  16.3 us
    all_to_all x1, waiting for transfers between devices, copy_for_each(): return lax.all_to_all(copies, axis, split_axis=0, concat_axis=0, tiled=True)  10.1 us
    all_to_all x2, starting transfers between devices, sum_at_owner(): lax.all_to_all(blocks, axis, split_axis=0, concat_axis=0, tiled=True)  9.48 us
    unnamed x52, local copies, waits for them, and re-layouts  9 us
    all_to_all x2, other arithmetic, sum_at_owner(): lax.all_to_all(blocks, axis, split_axis=0, concat_axis=0, tiled=True)  2.18 us
  transfers between devices with their start and end apart: 3, of which 3 were waited for; matrix products, arithmetic and copies ran while one was open for 2% of the time, Pallas kernels for 0%

commit v1 on v0

v1 whole, which is shorter than its diff:
```python
import jax
import jax.numpy as jnp
from jax import lax
from jax.experimental import pallas as pl
from jax.experimental.pallas import tpu as pltpu
from jax.sharding import PartitionSpec as P

F32 = jnp.float32
BF16 = jnp.bfloat16
NORM_EPS = 1e-05
SIDE = 8
NEAR = (1, 7, 2, 6, 3, 5, 4)
FAR = (4, 3, 5, 2, 6, 1, 7)
MESH = pl.DeviceIdType.MESH
NAMES = (
    "tokens",
    "mix_gain",
    "w_gate",
    "w_value",
    "w_maps",
    "w_step",
    "conv_value",
    "conv_maps",
    "past_value",
    "past_maps",
    "step_bias",
    "decay_log",
    "skip_gain",
    "head_gain",
    "state",
    "w_out",
    "mlp_gain",
    "w_up",
    "w_down",
)
ORDER = (
    "mix_gain",
    "w_maps",
    "w_gate",
    "w_value",
    "w_step",
    "past_value",
    "past_maps",
    "conv_value",
    "conv_maps",
    "step_bias",
    "decay_log",
    "skip_gain",
    "head_gain",
    "state",
    "w_out",
    "mlp_gain",
    "w_up",
    "w_down",
)


def silu(v):
    return v * (1.0 / (1.0 + jnp.exp(-v)))


def softplus(v):
    return jnp.maximum(v, 0.0) + jnp.log1p(jnp.exp(-jnp.abs(v)))


def dot(a, b):
    return lax.dot_general(a, b, (((1,), (0,)), ((), ())), preferred_element_type=F32)


def dot_t(a, b):
    return lax.dot_general(a, b, (((1,), (1,)), ((), ())), preferred_element_type=F32)


def kernel(*refs):
    n_in = len(NAMES)
    hbm = dict(zip(NAMES, refs[:n_in]))
    layer_out, state_next, value_tail, maps_tail = refs[n_in : n_in + 4]
    vm = dict(zip(NAMES, refs[n_in + 4 : 2 * n_in + 4]))
    (
        snext_buf, xbuf, xs, pbuf, r1, r2, hbuf, fbuf, f1, fpk, f2,
        load_sem, store_sem, a_s, a_r, s1, q1, s2, q2, s3, q3, s4, q4, s5, q5,
    ) = refs[2 * n_in + 4 :]

    me = lax.axis_index("kv")
    z = me // SIDE
    y = lax.rem(me, SIDE)

    def zpeer(d):
        return {"kv": lax.rem(z + d, SIDE) * SIDE + y}

    def ypeer(d):
        return {"kv": z * SIDE + lax.rem(y + d, SIDE)}

    def zsrc(d):
        return lax.rem(z + SIDE - d, SIDE)

    def ysrc(d):
        return lax.rem(y + SIDE - d, SIDE)

    def load(name):
        src = hbm[name]
        if name == "w_step":
            src = src.at[pl.ds(pl.multiple_of(z * SIDE, SIDE), SIDE), :]
        return pltpu.make_async_copy(src, vm[name], load_sem.at[NAMES.index(name)])

    sent = []

    def send(src, dst, ssem, rsem, peer):
        copy = pltpu.make_async_remote_copy(
            src_ref=src, dst_ref=dst, send_sem=ssem, recv_sem=rsem, device_id=peer, device_id_type=MESH
        )
        copy.start()
        sent.append(copy)

    def arrived(dst, ssem, rsem):
        pltpu.make_async_remote_copy(
            src_ref=dst, dst_ref=dst, send_sem=ssem, recv_sem=rsem, device_id=zpeer(1), device_id_type=MESH
        ).wait_recv()

    load("tokens").start()
    barrier = pltpu.get_barrier_semaphore()
    for d in FAR:
        pl.semaphore_signal(barrier, inc=1, device_id=zpeer(d), device_id_type=MESH)
        pl.semaphore_signal(barrier, inc=1, device_id=ypeer(d), device_id_type=MESH)
    for name in ORDER:
        load(name).start()

    lane = lax.broadcasted_iota(jnp.int32, (8, 128), 1)

    load("tokens").wait()
    own = vm["tokens"][...].astype(F32)
    packed = jnp.concatenate([own[0:8], own[8:16], own[16:24], jnp.zeros((8, 32), F32)], axis=1)
    xbuf[z, y] = packed.astype(BF16)
    pl.semaphore_wait(barrier, 14)
    for d in FAR:
        send(xbuf.at[z, y], xbuf.at[z, y], a_s.at[0, d], a_r.at[0, d], ypeer(d))
        send(xbuf.at[z, y], xbuf.at[z, y], a_s.at[d, 0], a_r.at[d, 0], zpeer(d))

    for name in ORDER[:11]:
        load(name).wait()
    conv_v = vm["conv_value"][...]
    conv_m = vm["conv_maps"][...]
    pre_v = sum(vm["past_value"][k].astype(F32) * conv_v[k : k + 1] for k in range(3))
    pre_m = sum(vm["past_maps"][k].astype(F32) * conv_m[k : k + 1] for k in range(3))
    for k in range(2):
        value_tail[k] = vm["past_value"][k + 1]
        maps_tail[k] = vm["past_maps"][k + 1]

    for dy in NEAR:
        block = xbuf.at[z, ysrc(dy)]
        arrived(block, a_s.at[0, dy], a_r.at[0, dy])
        for d in FAR:
            send(block, block, a_s.at[d, dy], a_r.at[d, dy], zpeer(d))

    sq = jnp.zeros((24, 128), F32)
    acc_g = jnp.zeros((24, 64), F32)
    acc_v = jnp.zeros((24, 64), F32)
    acc_s = jnp.zeros((24, 8), F32)
    acc_m = jnp.zeros((24, 256), F32)
    for dz in (0,) + NEAR:
        zi = zsrc(dz)
        if dz:
            for dy in range(SIDE):
                arrived(xbuf.at[zi, ysrc(dy)], a_s.at[dz, dy], a_r.at[dz, dy])
        halves = []
        for t in range(2):
            parts = []
            blocks = [xbuf[zi, 4 * t + j].astype(F32) for j in range(4)]
            for g in range(3):
                tile = None
                for j in range(4):
                    shift = (32 * j - 32 * g) % 128
                    moved = pltpu.roll(blocks[j], shift, 1) if shift else blocks[j]
                    tile = moved if tile is None else jnp.where(lane >= 32 * j, moved, tile)
                parts.append(tile)
            tile = jnp.concatenate(parts, axis=0)
            xs[2 * zi + t] = tile
            sq = sq + tile * tile
            halves.append((tile * vm["mix_gain"][pl.ds(2 * zi + t, 1), :]).astype(BF16))
        lhs = jnp.concatenate(halves, axis=1)
        cols = pl.ds(pl.multiple_of(zi * 256, 256), 256)
        acc_m = acc_m + dot(lhs, vm["w_maps"][cols, :])
        acc_g = acc_g + dot_t(lhs, vm["w_gate"][:, cols])
        acc_v = acc_v + dot_t(lhs, vm["w_value"][:, cols])
        acc_s = acc_s + dot_t(lhs, vm["w_step"][:, cols])

    inv = lax.rsqrt(jnp.sum(sq, axis=1, keepdims=True) * (1.0 / 2048.0) + NORM_EPS)
    gate_pre = acc_g * inv
    value_new = (acc_v * inv).astype(BF16)
    maps_new = (acc_m * inv).astype(BF16)
    value_tail[2] = value_new
    maps_tail[2] = maps_new
    step_lane = lax.broadcasted_iota(jnp.int32, (24, 8), 1)
    step_pre = jnp.sum(jnp.where(step_lane == y, acc_s, 0.0), axis=1, keepdims=True) * inv

    value_act = silu(pre_v + value_new.astype(F32) * conv_v[3:4])
    maps_act = silu(pre_m + maps_new.astype(F32) * conv_m[3:4]).astype(BF16).astype(F32)
    in_map = maps_act[:, :128]
    out_map = maps_act[:, 128:]
    step_size = softplus(step_pre + vm["step_bias"][...])
    decay = jnp.exp(-step_size * jnp.exp(vm["decay_log"][...]))

    load("state").wait()
    lane64 = lax.broadcasted_iota(jnp.int32, (64, 128), 1)
    reads = jnp.zeros((64, 128), F32)
    for b in range(24):
        total = jnp.sum(vm["state"][b] * out_map[b : b + 1, :], axis=1, keepdims=True)
        reads = jnp.where(lane64 == b, total, reads)
    old_read = jnp.transpose(jnp.concatenate([reads, jnp.zeros((64, 128), F32)], axis=0))[:24, :64]
    met = jnp.sum(in_map * out_map, axis=1, keepdims=True)
    load("skip_gain").wait()
    load("head_gain").wait()
    written = step_size * value_act
    read_out = decay * old_read + written * met + vm["skip_gain"][...] * value_act
    gated = read_out * silu(gate_pre)
    head_inv = lax.rsqrt(jnp.sum(gated * gated, axis=1, keepdims=True) * (1.0 / 64.0) + NORM_EPS)
    heads_out = (gated * head_inv * vm["head_gain"][...]).astype(BF16)

    load("w_out").wait()
    for c in range(16):
        pbuf[c] = dot(heads_out, vm["w_out"][:, c * 128 : c * 128 + 128]).astype(BF16)

    for d in FAR:
        send(pbuf.at[lax.rem(z + d, SIDE)], r1.at[0, d], s1.at[0, d], q1.at[0, d], zpeer(d))
        send(pbuf.at[8 + lax.rem(y + d, SIDE)], r1.at[1, d], s1.at[1, d], q1.at[1, d], ypeer(d))

    decay_rows = jnp.broadcast_to(decay, (24, 128))
    padded = jnp.concatenate([written, jnp.zeros((24, 64), F32)], axis=1)
    padded = jnp.concatenate([padded, jnp.zeros((104, 128), F32)], axis=0)
    columns = jnp.transpose(padded)[:64, :]
    for b in range(24):
        snext_buf[b] = (
            decay_rows[b : b + 1, :] * vm["state"][b] + columns[:, b : b + 1] * in_map[b : b + 1, :]
        )
    state_out = pltpu.make_async_copy(snext_buf, state_next, store_sem)
    state_out.start()
    for name in ORDER[-3:]:
        load(name).wait()

    sum_p = pbuf[z].astype(F32)
    sum_q = pbuf[8 + y].astype(F32)
    for d in NEAR:
        arrived(r1.at[0, d], s1.at[0, d], q1.at[0, d])
        sum_p = sum_p + r1[0, d].astype(F32)
        arrived(r1.at[1, d], s1.at[1, d], q1.at[1, d])
        sum_q = sum_q + r1[1, d].astype(F32)
    r2[0, y] = sum_p.astype(BF16)
    r2[1, z] = sum_q.astype(BF16)
    for d in FAR:
        send(r2.at[0, y], r2.at[0, y], s2.at[0, d], q2.at[0, d], ypeer(d))
        send(r2.at[1, z], r2.at[1, z], s2.at[1, d], q2.at[1, d], zpeer(d))
    for d in NEAR:
        arrived(r2.at[0, ysrc(d)], s2.at[0, d], q2.at[0, d])
        arrived(r2.at[1, zsrc(d)], s2.at[1, d], q2.at[1, d])
    sum_p = r2[0, 0].astype(F32)
    sum_q = r2[1, 0].astype(F32)
    for k in range(1, SIDE):
        sum_p = sum_p + r2[0, k].astype(F32)
        sum_q = sum_q + r2[1, k].astype(F32)
    hbuf[z] = (xs[z] + sum_p).astype(BF16)
    hbuf[8 + y] = (xs[8 + y] + sum_q).astype(BF16)
    for d in FAR:
        send(hbuf.at[z], hbuf.at[z], s3.at[0, d], q3.at[0, d], zpeer(d))
        send(hbuf.at[8 + y], hbuf.at[8 + y], s3.at[1, d], q3.at[1, d], ypeer(d))

    sq = jnp.zeros((24, 128), F32)
    up = jnp.zeros((24, 128), F32)
    for d in (0,) + NEAR:
        for half in range(2):
            c = zsrc(d) if half == 0 else 8 + ysrc(d)
            if d:
                arrived(hbuf.at[c], s3.at[half, d], q3.at[half, d])
            h = hbuf[c].astype(F32)
            sq = sq + h * h
            scaled = (h * vm["mlp_gain"][pl.ds(c, 1), :]).astype(BF16)
            up = up + dot(scaled, vm["w_up"][pl.ds(pl.multiple_of(c * 128, 128), 128), :])
    inv = lax.rsqrt(jnp.sum(sq, axis=1, keepdims=True) * (1.0 / 2048.0) + NORM_EPS)
    relu = jnp.maximum(up * inv, 0.0)
    squared = (relu * relu).astype(BF16)
    for c in range(16):
        fbuf[c // 2, c % 2] = dot(squared, vm["w_down"][:, c * 128 : c * 128 + 128]).astype(BF16)

    for d in FAR:
        send(fbuf.at[lax.rem(z + d, SIDE)], f1.at[d], s4.at[d], q4.at[d], zpeer(d))
    total = fbuf[z].astype(F32)
    for d in NEAR:
        arrived(f1.at[d], s4.at[d], q4.at[d])
        total = total + f1[d].astype(F32)
    for t in range(2):
        for j in range(4):
            tile = None
            for g in range(3):
                shift = (32 * g - 32 * j) % 128
                rows = total[t, 8 * g : 8 * g + 8, :]
                moved = pltpu.roll(rows, shift, 1) if shift else rows
                tile = moved if tile is None else jnp.where(lane >= 32 * g, moved, tile)
            fpk[4 * t + j] = tile.astype(BF16)
    for d in FAR:
        send(fpk.at[lax.rem(y + d, SIDE)], f2.at[d], s5.at[d], q5.at[d], ypeer(d))
    total = fpk[y].astype(F32)
    for d in NEAR:
        arrived(f2.at[d], s5.at[d], q5.at[d])
        total = total + f2[d].astype(F32)
    mlp = jnp.concatenate(
        [total[:, :32], pltpu.roll(total, 96, 1)[:, :32], pltpu.roll(total, 64, 1)[:, :32]], axis=0
    )
    near_cols = hbuf[2 * z + y // 4].astype(F32)
    own_hidden = pltpu.roll(near_cols, lax.rem(128 - 32 * lax.rem(y, 4), 128), 1)[:, :32]
    layer_out[...] = (own_hidden + mlp).astype(BF16)

    for copy in sent:
        copy.wait_send()
    state_out.wait()


def local(
    tokens, mix_gain, w_gate, w_value, w_maps, w_step, conv_value, conv_maps, past_value, past_maps,
    step_bias, decay_log, skip_gain, head_gain, state, w_out, mlp_gain, w_up, w_down,
):
    args = (
        tokens,
        mix_gain.reshape(16, 128),
        w_gate.T,
        w_value.T,
        w_maps,
        w_step.T,
        conv_value,
        conv_maps,
        jnp.transpose(past_value, (1, 0, 2)),
        jnp.transpose(past_maps, (1, 0, 2)),
        step_bias.reshape(1, 1),
        decay_log.reshape(1, 1),
        skip_gain.reshape(1, 1),
        head_gain.reshape(1, 64),
        state.reshape(24, 64, 128),
        w_out,
        mlp_gain.reshape(16, 128),
        w_up,
        w_down,
    )
    buffers = []
    for k, a in enumerate(args):
        shape = (SIDE, 2048) if k == 5 else a.shape
        buffers.append(pltpu.VMEM(shape, a.dtype))
    dma = pltpu.SemaphoreType.DMA
    layer_out, state_next, value_tail, maps_tail = pl.pallas_call(
        kernel,
        out_shape=(
            jax.ShapeDtypeStruct((24, 32), BF16),
            jax.ShapeDtypeStruct((24, 64, 128), F32),
            jax.ShapeDtypeStruct((3, 24, 64), BF16),
            jax.ShapeDtypeStruct((3, 24, 256), BF16),
        ),
        in_specs=[pl.BlockSpec(memory_space=pltpu.HBM)] * len(args),
        out_specs=(
            pl.BlockSpec(memory_space=pltpu.VMEM),
            pl.BlockSpec(memory_space=pltpu.HBM),
            pl.BlockSpec(memory_space=pltpu.VMEM),
            pl.BlockSpec(memory_space=pltpu.VMEM),
        ),
        scratch_shapes=buffers
        + [
            pltpu.VMEM((24, 64, 128), F32),
            pltpu.VMEM((SIDE, SIDE, 8, 128), BF16),
            pltpu.VMEM((16, 24, 128), F32),
            pltpu.VMEM((16, 24, 128), BF16),
            pltpu.VMEM((2, SIDE, 24, 128), BF16),
            pltpu.VMEM((2, SIDE, 24, 128), BF16),
            pltpu.VMEM((16, 24, 128), BF16),
            pltpu.VMEM((SIDE, 2, 24, 128), BF16),
            pltpu.VMEM((SIDE, 2, 24, 128), BF16),
            pltpu.VMEM((SIDE, 8, 128), BF16),
            pltpu.VMEM((SIDE, 8, 128), BF16),
            dma((len(args),)),
            dma,
            dma((SIDE, SIDE)),
            dma((SIDE, SIDE)),
            dma((2, SIDE)),
            dma((2, SIDE)),
            dma((2, SIDE)),
            dma((2, SIDE)),
            dma((2, SIDE)),
            dma((2, SIDE)),
            dma((SIDE,)),
            dma((SIDE,)),
            dma((SIDE,)),
            dma((SIDE,)),
        ],
        compiler_params=pltpu.CompilerParams(collective_id=0, has_side_effects=True, vmem_limit_bytes=67043328),
        name="layer",
    )(*args)
    return (
        layer_out,
        state_next.reshape(24, 1, 64, 128),
        jnp.transpose(value_tail, (1, 0, 2)),
        jnp.transpose(maps_tail, (1, 0, 2)),
    )


def solution(mesh):
    rows = ("dp", "tp")
    in_specs = (
        P(rows, "kv"),
        P(),
        P(None, "kv"),
        P(None, "kv"),
        P(None, "kv"),
        P(),
        P(None, "kv"),
        P(None, "kv"),
        P(rows, None, "kv"),
        P(rows, None, "kv"),
        P("kv"),
        P("kv"),
        P("kv"),
        P("kv"),
        P(rows, "kv", None, None),
        P("kv", None),
        P(),
        P(None, "kv"),
        P("kv", None),
    )
    out_specs = (
        P(rows, "kv"),
        P(rows, "kv", None, None),
        P(rows, None, "kv"),
        P(rows, None, "kv"),
    )
    return jax.shard_map(local, mesh=mesh, in_specs=in_specs, out_specs=out_specs, check_vma=False)
```

time: 103 us -> 59 us (0.57)
  Pallas kernels: 0 us -> 51.3 us
  waiting for transfers between devices: 35 us -> 0 us
  starting transfers between devices: 26.1 us -> 0 us
  blocking collectives: 16.3 us -> 0 us
  local copies, waits for them, and re-layouts: 13.9 us -> 4.77 us
  other arithmetic: 5.82 us -> 0 us
  matrix products: 2.58 us -> 0 us
    pallas_call x0 -> x1, Pallas kernels: none -> 51.3 us  [local(): pl.pallas_call(kernel, out_shape=(jax.ShapeDtypeStruct((24, 32), BF16), j...]
    all_to_all x3 -> x0, waiting for transfers between devices: 35 us -> none  [the longest x2 24.9 us: sum_at_owner(): lax.all_to_all(blocks, axis, split_axis=0, concat_axis=0, tiled=True)]
    all_to_all x3 -> x0, starting transfers between devices: 26.1 us -> none  [the longest x1 16.6 us: copy_for_each(): return lax.all_to_all(copies, axis, split_axis=0, concat_axis=0, tiled=True)]
    all_to_all x1 -> x0, blocking collectives: 16.3 us -> none  [copy_for_each(): return lax.all_to_all(copies, axis, split_axis=0, concat_axis=0, tiled=True)]
    unnamed x52 -> x10, local copies, waits for them, and re-layouts: 9 us -> 4.77 us
    dot_general x6 -> x0, matrix products: 2.58 us -> none  [the longest x1 0.91 us: local(): step_pre = jnp.dot(normed, step_cols, preferred_element_type=jnp.float32)]
    all_to_all x2 -> x0, other arithmetic: 2.18 us -> none  [sum_at_owner(): lax.all_to_all(blocks, axis, split_axis=0, concat_axis=0, tiled=True)]
    convert_element_type x5 -> x0, local copies, waits for them, and re-layouts: 2.1 us -> none  [the longest x4 1.05 us: rms_rows(): widened = matrix.astype(jnp.float32)]
  transfers between devices with their start and end apart: 3 -> 0, of which waited for: 3 -> 0; matrix products, arithmetic and copies ran while one was open for 2% -> 0% of each run, Pallas kernels for 0% -> 0%
where the time goes in v1:
time: 59 us; the launch traced here: 58.7 us
  Pallas kernels  51.3 us (87%)
  local copies, waits for them, and re-layouts  4.77 us (8%)
  between operations  2.59 us (4%)
    pallas_call x1, Pallas kernels, local(): pl.pallas_call(kernel, out_shape=(jax.ShapeDtypeStruct((24, 32), BF16), j...  51.3 us
    unnamed x10, local copies, waits for them, and re-layouts  4.77 us

profile of v1, /device:TPU:6, one launch (start us, length us, event | category | flops | bytes accessed | tf_op | source)
XLA Modules:
  0.0 58.7 jit_solution(4301128760517269888)
XLA Ops:
  2.6 51.3 %layer.1 = (bf16[24,32]{1,0:T(8,128)(2,1)}, f32[24,64,128]{2,1,0:T(8,128)}, bf16[3,24,64]{2,1,0:T(8,128)(2,1)}, bf16[3,24,256]{2,1,0:T(8,128)(2,1)}) custom-call(bf16[24,32]{1,0:T(8,128)(2,1)} %refs_0_.1, f32[16,128]{1,0:T(8,128)} %bitcast.29, bf16[64,2048]{1,0:T(8,128)(2,1)} %bitcast.22, bf16[64,2048]{1,0:T(8,128)(2,1)} %bitcast.23, ...), custom_call_target="tpu_custom_call" | custom-call | tf_op jit(solution)/shard_map/layer/pallas_call | solution.py:346
  53.9 0.0 copy-start.2
  53.9 0.7 %copy-done.2 = bf16[24,32]{1,0:T(8,128)(2,1)S(1)} copy-done((bf16[24,32]{1,0:T(8,128)(2,1)S(1)}, bf16[24,32]{1,0:T(8,128)(2,1)}, u32[]{:S(2)}) %copy-start.2) | copy-done | bytes 1560
  54.6 0.6 %copy.31 = bf16[24,32]{1,0:T(8,128)(2,1)} copy(bf16[24,32]{1,0:T(8,128)(2,1)S(1)} %copy-done.2) | data formatting | bytes 3072
  55.2 0.0 copy-start.1
  55.2 2.1 %copy.32 = f32[24,1,64,128]{3,2,1,0:T(8,128)} copy(f32[24,1,64,128]{3,2,1,0:T(8,128)} %bitcast.20) | data formatting | bytes 1572864
  57.3 0.0 copy-done.1
  57.3 0.0 copy-start
  57.3 0.6 %copy.33 = bf16[24,3,64]{2,0,1:T(8,128)(2,1)} copy(bf16[24,3,64]{2,0,1:T(8,128)(2,1)S(1)} %bitcast.28) | data formatting | bytes 18432
  57.9 0.2 copy-done
  58.1 0.6 %copy.34 = bf16[24,3,256]{2,0,1:T(8,128)(2,1)} copy(bf16[24,3,256]{2,0,1:T(8,128)(2,1)S(1)} %bitcast.26) | data formatting | bytes 73728
Async XLA Ops:
  53.9 0.7 %copy-start.2 = (bf16[24,32]{1,0:T(8,128)(2,1)S(1)}, bf16[24,32]{1,0:T(8,128)(2,1)}, u32[]{:S(2)}) copy-start(bf16[24,32]{1,0:T(8,128)(2,1)} %get-tuple-element.20) | copy-start | bytes 4612
  55.2 2.1 %copy-start.1 = (bf16[3,24,64]{2,1,0:T(8,128)(2,1)S(1)}, bf16[3,24,64]{2,1,0:T(8,128)(2,1)}, u32[]{:S(2)}) copy-start(bf16[3,24,64]{2,1,0:T(8,128)(2,1)} %get-tuple-element.10) | copy-start | bytes 27652
  57.3 0.8 %copy-start = (bf16[3,24,256]{2,1,0:T(8,128)(2,1)S(1)}, bf16[3,24,256]{2,1,0:T(8,128)(2,1)}, u32[]{:S(2)}) copy-start(bf16[3,24,256]{2,1,0:T(8,128)(2,1)} %get-tuple-element.11) | copy-start | bytes 110596

commit v2 on v1

--- a/solution.py
+++ b/solution.py
@@ -77,8 +77,8 @@
     layer_out, state_next, value_tail, maps_tail = refs[n_in : n_in + 4]
     vm = dict(zip(NAMES, refs[n_in + 4 : 2 * n_in + 4]))
     (
-        snext_buf, xbuf, xs, pbuf, r1, r2, hbuf, fbuf, f1, fpk, f2,
-        load_sem, store_sem, a_s, a_r, s1, q1, s2, q2, s3, q3, s4, q4, s5, q5,
+        xbuf, xs, pbuf, r1, r2, hbuf, fbuf, f1, fpk, f2,
+        load_sem, a_s, a_r, s1, q1, s2, q2, s3, q3, s4, q4, s5, q5,
     ) = refs[2 * n_in + 4 :]
 
     me = lax.axis_index("kv")
@@ -229,11 +229,9 @@
     padded = jnp.concatenate([padded, jnp.zeros((104, 128), F32)], axis=0)
     columns = jnp.transpose(padded)[:64, :]
     for b in range(24):
-        snext_buf[b] = (
+        state_next[b] = (
             decay_rows[b : b + 1, :] * vm["state"][b] + columns[:, b : b + 1] * in_map[b : b + 1, :]
         )
-    state_out = pltpu.make_async_copy(snext_buf, state_next, store_sem)
-    state_out.start()
     for name in ORDER[-3:]:
         load(name).wait()
 
@@ -310,7 +308,14 @@
 
     for copy in sent:
         copy.wait_send()
-    state_out.wait()
+
+
+def hand_over(*refs):
+    copies = [pltpu.make_async_copy(refs[k], refs[4 + k], refs[8].at[k]) for k in range(4)]
+    for copy in copies:
+        copy.start()
+    for copy in copies:
+        copy.wait()
 
 
 def local(
@@ -354,13 +359,12 @@
         in_specs=[pl.BlockSpec(memory_space=pltpu.HBM)] * len(args),
         out_specs=(
             pl.BlockSpec(memory_space=pltpu.VMEM),
-            pl.BlockSpec(memory_space=pltpu.HBM),
+            pl.BlockSpec(memory_space=pltpu.VMEM),
             pl.BlockSpec(memory_space=pltpu.VMEM),
             pl.BlockSpec(memory_space=pltpu.VMEM),
         ),
         scratch_shapes=buffers
         + [
-            pltpu.VMEM((24, 64, 128), F32),
             pltpu.VMEM((SIDE, SIDE, 8, 128), BF16),
             pltpu.VMEM((16, 24, 128), F32),
             pltpu.VMEM((16, 24, 128), BF16),
@@ -372,7 +376,6 @@
             pltpu.VMEM((SIDE, 8, 128), BF16),
             pltpu.VMEM((SIDE, 8, 128), BF16),
             dma((len(args),)),
-            dma,
             dma((SIDE, SIDE)),
             dma((SIDE, SIDE)),
             dma((2, SIDE)),
@@ -386,9 +389,18 @@
             dma((SIDE,)),
             dma((SIDE,)),
         ],
-        compiler_params=pltpu.CompilerParams(collective_id=0, has_side_effects=True, vmem_limit_bytes=67043328),
+        compiler_params=pltpu.CompilerParams(collective_id=0, has_side_effects=True, vmem_limit_bytes=48 * 2**20),
         name="layer",
-    )(*args)
+    )(*[a if a.size == 1 else pltpu.with_memory_space_constraint(a, pltpu.HBM) for a in args])
+    layer_out, state_next, value_tail, maps_tail = pl.pallas_call(
+        hand_over,
+        out_shape=tuple(jax.ShapeDtypeStruct(o.shape, o.dtype) for o in (layer_out, state_next, value_tail, maps_tail)),
+        in_specs=[pl.BlockSpec(memory_space=pltpu.VMEM)] * 4,
+        out_specs=(pl.BlockSpec(memory_space=pltpu.HBM),) * 4,
+        scratch_shapes=[dma((4,))],
+        compiler_params=pltpu.CompilerParams(vmem_limit_bytes=8 * 2**20),
+        name="hand_over",
+    )(layer_out, state_next, value_tail, maps_tail)
     return (
         layer_out,
         state_next.reshape(24, 1, 64, 128),

time: 59 us -> 54.3 us (0.920)
  local copies, waits for them, and re-layouts: 4.77 us -> 0 us
    unnamed x10 -> x0, local copies, waits for them, and re-layouts: 4.77 us -> none
    pallas_call x0 -> x1, Pallas kernels: none -> 0.93 us  [local(): pl.pallas_call(hand_over, out_shape=tuple((jax.ShapeDtypeStruct(o.shape,...]
    pallas_call x1, Pallas kernels: 51.3 us -> 50.7 us  [local(): pl.pallas_call(kernel, out_shape=(jax.ShapeDtypeStruct((24, 32), BF16), j...]
where the time goes in v2:
time: 54.3 us; the launch traced here: 54.2 us
  Pallas kernels  51.6 us (95%)
  between operations  2.58 us (5%)
    pallas_call x1, Pallas kernels, local(): pl.pallas_call(kernel, out_shape=(jax.ShapeDtypeStruct((24, 32), BF16), j...  50.7 us

profile of v2, /device:TPU:6, one launch (start us, length us, event | category | flops | bytes accessed | tf_op | source)
XLA Modules:
  0.0 54.2 jit_solution(13660581618291418979)
XLA Ops:
  2.6 50.7 %layer.1 = (bf16[24,32]{1,0:T(8,128)(2,1)S(1)}, f32[24,64,128]{2,1,0:T(8,128)S(1)}, bf16[3,24,64]{2,1,0:T(8,128)(2,1)S(1)}, bf16[3,24,256]{2,1,0:T(8,128)(2,1)S(1)}) custom-call(bf16[24,32]{1,0:T(8,128)(2,1)} %refs_0_.1, f32[16,128]{1,0:T(8,128)} %bitcast.26, bf16[64,2048]{1,0:T(8,128)(2,1)} %bitcast.21, bf16[64,2048]{1,0:T(8,128)(2,1)} %bitcast.22, ...), custom_call_target="tpu_custom_call" | custom-call | tf_op jit(solution)/shard_map/layer/pallas_call | solution.py:351
  53.2 0.9 %hand_over.1 = (bf16[24,32]{1,0:T(8,128)(2,1)}, f32[24,64,128]{2,1,0:T(8,128)}, bf16[3,24,64]{2,1,0:T(8,128)(2,1)}, bf16[3,24,256]{2,1,0:T(8,128)(2,1)}) custom-call(bf16[24,32]{1,0:T(8,128)(2,1)S(1)} %get-tuple-element.12.refs_0_, f32[24,64,128]{2,1,0:T(8,128)S(1)} %get-tuple-element.13.refs_1_, bf16[3,24,64]{2,1,0:T(8,128)(2,1)S(1)} %get-tuple-element.14.refs_2_, ...), custom_call_target="tpu_custom_call" | custom-call | tf_op jit(solution)/shard_map/hand_over/pallas_call | solution.py:395
